TPU v7x, 32 devices: a whole 2x2x4 slice. The times are simulated.
32 devices in a mesh: ep: 8 (over z, x), tp: 4 (over y, core).
Axes of the slice: x: 2, y: 2, z: 4, core: 2. Of those that a mesh axis runs over, the one named last changes fastest.
Arguments:
- query_logits: bfloat16 [2048, 2048], P('ep', 'tp'), may hold values from -6 to 6
- forget_gate_logits: bfloat16 [2048, 2048], P('ep', 'tp'), may hold values from -3.75 to 3.75
- written_values: bfloat16 [2048, 2048], P('ep', 'tp'), may hold values from -6 to 6
- output_gate_logits: bfloat16 [2048, 2048], P('ep', 'tp'), may hold values from -6 to 6
- gap: float32 [2048], P('tp'), may hold values from 4.8828125e-05 to 0.06
- extra_log_forget: float32 [2048, 2048], P('ep', 'tp'), may hold values from -0.7 to 0
- head_norm_scale: float32 [2048], P('tp'), may hold values from 0.1 to 1.9
- mixer_output_matrix: bfloat16 [2048, 2048], P('tp'), may hold values from -0.125 to 0.125
- expert_input_tokens: bfloat16 [2048, 2048], P('ep'), may hold values from -12 to 12
- expert_norm_scale: float32 [2048], replicated, may hold values from 0.1 to 1.9
- routes: int32 [2048, 2], P('ep'), may hold values from 0 to 7, all different within a row; in each aligned block of 256 rows (0 to 255, 256 to 511, ...) at most 96 rows name the same one
- router_scores_chosen: float32 [2048, 2], P('ep'), may hold values from -6 to 6
- expert_gate_matrix: bfloat16 [8, 2048, 4096], P('ep', None, 'tp'), may hold values from -0.125 to 0.125
- expert_up_matrix: bfloat16 [8, 2048, 4096], P('ep', None, 'tp'), may hold values from -0.125 to 0.125
- expert_down_matrix: bfloat16 [8, 2048, 4096], P('ep', None, 'tp'), may hold values from -0.09375 to 0.09375
Outputs:
- mixer_output_rows: bfloat16 [2048, 2048], P(('ep', 'tp'))
- expert_out: bfloat16 [2048, 2048], P('ep', 'tp')
Inputs may be any that keep to these rules, and one draw needn't show every extreme that they name: `routes`: each row names two different experts. Among the rows of one device no expert is named more than 96 times, and 96 is reached in some blocks.
All inputs are finite; a program needn't handle non-finite values.
Results may differ from a plain program's by a relative error of at most 0.019.
Values may be sent and summed in bfloat16 or wider, within the bound.
A program may use at most 64 MiB of HBM per device.

v0:
```python
import jax
import jax.numpy as jnp
from jax import lax
from jax.sharding import PartitionSpec as P

HEAD_DIM = 128
exact_precision = lax.Precision.HIGHEST


def entering(x, axis, join, neutral):
    place = lax.axis_index(axis)
    gathered = jax.tree.map(
        lambda a, kind: lax.all_gather(a.astype(kind), axis), x, (jnp.bfloat16, jnp.bfloat16)
    )
    state = jax.tree.map(lambda a, e: jnp.zeros_like(a) + jnp.asarray(e, a.dtype), x, neutral)

    def one(hop, state):
        return join(
            state,
            jax.tree.map(
                lambda a, own: lax.dynamic_index_in_dim(a, hop, 0, False).astype(own.dtype),
                gathered,
                x,
            ),
        )

    return lax.fori_loop(0, place, one, state)


def join_states(earlier, later):
    decay_early, state_early = earlier
    decay_late, state_late = later
    return (decay_early * decay_late, decay_late[..., None] * state_early + state_late)


def mixer_half(
    query_logits,
    forget_gate_logits,
    written_values,
    output_gate_logits,
    gap,
    extra_log_forget,
    head_norm_scale,
    mixer_output_matrix,
):
    tokens, channels = query_logits.shape
    local_heads = channels // HEAD_DIM
    final_result = gap * jax.nn.sigmoid(-forget_gate_logits.astype(jnp.float32))
    decay_logarithm = jnp.log1p(-final_result) + extra_log_forget
    queries = jax.nn.silu(query_logits.astype(jnp.float32))
    values = written_values.astype(jnp.float32)

    def by_head(array):
        return array.reshape(tokens, local_heads, HEAD_DIM).transpose(1, 0, 2)

    final_result, decay_logarithm, queries, values = (
        by_head(final_result),
        by_head(decay_logarithm),
        by_head(queries),
        by_head(values),
    )
    running = jnp.cumsum(decay_logarithm, axis=1)
    query_decayed = queries * jnp.exp(running)
    key_decayed = final_result * jnp.exp(-running)
    scores = jnp.einsum("htd,hsd->hts", query_decayed, key_decayed, precision=exact_precision)
    causal = jnp.arange(tokens)[:, None] >= jnp.arange(tokens)[None, :]
    scores = jnp.where(causal[None], scores, 0.0)
    within = jnp.einsum("hts,hsv->htv", scores, values, precision=exact_precision)
    ending = running[:, -1:, :]
    key_state = final_result * jnp.exp(ending - running)
    end_state = jnp.einsum("htd,htv->hdv", key_state, values, precision=exact_precision)
    span_decay = jnp.exp(ending[:, 0, :])
    identity = (jnp.ones_like(span_decay), jnp.zeros_like(end_state))
    _, incoming = entering((span_decay, end_state), "ep", join_states, identity)
    carried = jnp.einsum("htd,hdv->htv", query_decayed, incoming, precision=exact_precision)
    recurrent = within + carried
    scaled = recurrent * lax.rsqrt(jnp.mean(recurrent * recurrent, axis=-1, keepdims=True) + 1e-06)
    scaled = scaled.transpose(1, 0, 2).reshape(tokens, channels)
    hidden = (
        scaled * head_norm_scale * jax.nn.silu(output_gate_logits.astype(jnp.float32))
    ).astype(jnp.bfloat16)
    return lax.psum_scatter(
        jnp.dot(hidden, mixer_output_matrix, preferred_element_type=jnp.float32).astype(
            jnp.bfloat16
        ),
        "tp",
        scatter_dimension=0,
        tiled=True,
    )


def expert_half(
    expert_input_tokens,
    expert_norm_scale,
    routes,
    router_scores_chosen,
    expert_gate_matrix,
    expert_up_matrix,
    expert_down_matrix,
):
    tokens, channels = expert_input_tokens.shape
    experts = lax.axis_size("ep")
    capacity = 3 * tokens // experts
    inputs32 = expert_input_tokens.astype(jnp.float32)
    centred = inputs32 - jnp.mean(inputs32, axis=-1, keepdims=True)
    variance = jnp.mean(centred * centred, axis=-1, keepdims=True)
    normed = (centred * lax.rsqrt(variance + 1e-05) * expert_norm_scale).astype(jnp.bfloat16)
    first_weight = jax.nn.sigmoid(router_scores_chosen[:, 0] - router_scores_chosen[:, 1])
    route_weight = jnp.stack([first_weight, 1.0 - first_weight], axis=1)
    flat_routes = routes.reshape(-1)
    onehot = (flat_routes[:, None] == jnp.arange(experts, dtype=jnp.int32)[None, :]).astype(
        jnp.int32
    )
    earlier = jnp.cumsum(onehot, axis=0) - onehot
    position = jnp.sum(earlier * onehot, axis=1)
    target = flat_routes * capacity + position
    token_ids = jnp.arange(2 * tokens, dtype=jnp.int32) // 2
    owner = jnp.zeros((experts * capacity,), jnp.int32).at[target].set(token_ids)
    filled = jnp.zeros((experts * capacity,), jnp.bool_).at[target].set(True)
    local_gate = expert_gate_matrix[0]
    local_up = expert_up_matrix[0]
    local_down = expert_down_matrix[0]
    slice_width = channels // lax.axis_size("tp")
    own_columns = lax.dynamic_slice_in_dim(
        normed, lax.axis_index("tp") * slice_width, slice_width, 1
    )
    outgoing = jnp.where(filled[:, None], own_columns[owner], jnp.zeros((), jnp.bfloat16))
    arrived = lax.all_to_all(outgoing, "ep", split_axis=0, concat_axis=0, tiled=True)
    features = lax.all_gather(arrived, "tp", axis=1, tiled=True)
    gate_act = jnp.dot(features, local_gate, preferred_element_type=jnp.float32)
    up_act = jnp.dot(features, local_up, preferred_element_type=jnp.float32)
    hidden = (jax.nn.silu(gate_act) * up_act).astype(jnp.bfloat16)
    summed = lax.psum_scatter(
        lax.dot_general(
            local_down, hidden, (((1,), (1,)), ((), ())), preferred_element_type=jnp.float32
        ).astype(jnp.bfloat16),
        "tp",
        scatter_dimension=0,
        tiled=True,
    )
    returned = lax.all_to_all(summed, "ep", split_axis=1, concat_axis=1, tiled=True)
    chosen = returned.T[target].astype(jnp.float32).reshape(tokens, 2, -1)
    return jnp.sum(chosen * route_weight[:, :, None], axis=1).astype(jnp.bfloat16)


def body(
    query_logits,
    forget_gate_logits,
    written_values,
    output_gate_logits,
    gap,
    extra_log_forget,
    head_norm_scale,
    mixer_output_matrix,
    expert_input_tokens,
    expert_norm_scale,
    routes,
    router_scores_chosen,
    expert_gate_matrix,
    expert_up_matrix,
    expert_down_matrix,
):
    mixer_output_rows = mixer_half(
        query_logits,
        forget_gate_logits,
        written_values,
        output_gate_logits,
        gap,
        extra_log_forget,
        head_norm_scale,
        mixer_output_matrix,
    )
    expert_out = expert_half(
        expert_input_tokens,
        expert_norm_scale,
        routes,
        router_scores_chosen,
        expert_gate_matrix,
        expert_up_matrix,
        expert_down_matrix,
    )
    return (mixer_output_rows, expert_out)


def solution(mesh):
    return jax.shard_map(
        body,
        mesh=mesh,
        in_specs=(
            P("ep", "tp"),
            P("ep", "tp"),
            P("ep", "tp"),
            P("ep", "tp"),
            P("tp"),
            P("ep", "tp"),
            P("tp"),
            P("tp", None),
            P("ep", None),
            P(),
            P("ep", None),
            P("ep", None),
            P("ep", None, "tp"),
            P("ep", None, "tp"),
            P("ep", None, "tp"),
        ),
        out_specs=(P(("ep", "tp"), None), P("ep", "tp")),
        check_vma=False,
    )
```

profile of v0, /device:TPU:0, one launch (start us, length us, event | category | flops | bytes accessed | tf_op | source)
XLA Modules:
  0.0 200.6 jit_solution(9134592011714128732)
XLA Ops:
  7.2 0.9 copy.110
  8.2 0.1 eq.29
  8.3 0.1 eq.25
  8.5 0.7 broadcast_multiply_fusion
  9.2 1.4 convert_reduce_fusion
  10.6 2.9 %multiply_reduce_fusion = (f32[256]{0:T(256)S(1)}, f32[256,2048]{1,0:T(8,128)}) fusion(f32[256]{0:T(256)S(1)} %broadcast_multiply_fusion.1, bf16[256,2048]{1,0:T(8,128)(2,1)} %param.25), kind=kLoop, calls=%fused_computation.18 | loop fusion | flops 2096896 | bytes 3147776 | tf_op jit(solution)/shard_map/reduce_sum | solution.py:106
  13.5 1.1 reduce-window.16
  14.7 0.2 slice_reduce_fusion
  15.1 0.1 mul.131
  15.3 2.4 %scatter_custom_fusion.1 = s32[768]{0:T(1024)S(1)} fusion(s32[512]{0:T(512)S(1)} %bitcast.121, s32[512]{0:T(512)S(1)} %add_select_fusion, s32[]{:T(128)} %constant.71.clone.1), kind=kCustom, calls=%fused_computation.80 | custom fusion | bytes 3076 | tf_op jit(solution)/shard_map/scatter | solution.py:118
  17.8 2.4 %scatter_custom_fusion = pred[768]{0:T(1024)(128)(4,1)S(1)} fusion(s32[512]{0:T(512)S(1)} %bitcast.122, pred[512]{0:T(512)(128)(4,1)S(1)} %broadcast.132, pred[]{:T(512)} %constant.76.clone.1), kind=kCustom, calls=%fused_computation.84 | custom fusion | bytes 769 | tf_op jit(solution)/shard_map/scatter | solution.py:119
  20.4 0.8 dynamic-slice
  21.1 1.1 fusion.22
  22.3 2.7 %gather_fusion = bf16[768,512]{1,0:T(8,128)(2,1)S(1)} fusion(bf16[256,512]{1,0:T(8,128)(2,1)S(1)} %fusion.22, s32[1024]{0:T(1024)S(1)} %pad_clamp_fusion.1), kind=kCustom, calls=%fused_computation | custom fusion | bytes 1575936 | tf_op jit(solution)/shard_map/gather | solution.py:127
  25.0 0.2 broadcast_select_fusion
  25.2 27.3 %all_to_all.21 = bf16[8,96,512]{2,1,0:T(8,128)(2,1)} all-to-all(bf16[8,96,512]{2,1,0:T(8,128)(2,1)S(1)} %broadcast_select_fusion), channel_id=1, replica_groups=mesh['ep'=8,'tp'=4] {'ep'}, dimensions={0} | all-to-all | bytes 1572864 | tf_op jit(solution)/shard_map/all_to_all | solution.py:128
  52.6 1.2 copy.94
  53.8 1.1 copy.93
  54.9 1.1 divide_multiply_fusion
  56.1 0.2 copy.95
  56.3 0.4 fusion.25
  56.7 0.2 broadcast_add_fusion
  57.0 1.1 copy.146
  58.1 2.1 %copy.99 = f32[256,4,128]{2,1,0:T(4,128)} copy(f32[256,4,128]{0,2,1:T(8,128)} %bitcast.115) | data formatting | bytes 1048576 | tf_op jit(solution)/shard_map/reshape | solution.py:54
  60.3 1.8 copy.91
  62.1 1.1 convert_multiply_fusion.1
  63.2 1.0 copy.92
  64.2 0.7 slice_bitcast_fusion.1
  64.9 2.7 %bitcast_multiply_fusion.3 = (f32[4,256,128]{2,0,1:T(4,128)}, f32[4,256,128]{2,0,1:T(4,128)S(1)}, f32[4,256,128]{2,0,1:T(4,128)S(1)}) fusion(f32[256,4,128]{2,1,0:T(4,128)} %copy.99, f32[4,128,256]{1,2,0:T(8,128)S(1)} %bitcast.110, f32[4,128]{1,0:T(4,128)S(1)} %get-tuple-element.64, f32[256,4,128]{2,1,0:T(4,128)} %copy.92), kind=kLoop, calls=%fused_computation.41 | loop fusion | flops 655360 | bytes 3147776 | tf_op jit(solution)/shard_map/mul | solution.py:64
  67.6 1.3 convolution_convert_fusion.1
  68.9 0.2 reduce-scatter.5.cloned.1.call-start
  69.1 11.1 %all-gather.5.cloned.1.call-done = bf16[768,2048]{1,0:T(8,128)(2,1)} async-done(((bf16[768,512]{1,0:T(8,128)(2,1)}), bf16[768,2048]{1,0:T(8,128)(2,1)}) %all-gather.5.cloned.1.call-update) | async-done | bytes 3145744 | tf_op jit(solution)/shard_map/all_gather | solution.py:129
  80.2 6.3 %fusion.2 = f32[768,1024]{1,0:T(8,128)S(1)} fusion(bf16[768,2048]{1,0:T(8,128)(2,1)} %all-gather.5.cloned.1.call-done, bf16[1,2048,1024]{2,1,0:T(8,128)(2,1)} %param.30), kind=kOutput, calls=%fused_computation.8 | convolution fusion | flops 3221225472 | bytes 10485760 | tf_op jit(solution)/shard_map/dot_general | solution.py:131
  86.6 3.8 %multiply_convert_fusion = bf16[768,1024]{1,0:T(8,128)(2,1)S(1)} fusion(f32[768,1024]{1,0:T(8,128)S(1)} %fusion.2, bf16[768,2048]{1,0:T(8,128)(2,1)S(1)} %copy-done.9, bf16[1,2048,1024]{2,1,0:T(8,128)(2,1)S(1)} %copy-done.7), kind=kOutput, calls=%fused_computation.13 | convolution fusion | flops 3225944064 | bytes 12058624 | tf_op jit(solution)/shard_map/dot_general | solution.py:130
  90.4 4.9 %fusion.9 = bf16[2048,768]{0,1:T(8,128)(2,1)} fusion(bf16[768,1024]{1,0:T(8,128)(2,1)S(1)} %multiply_convert_fusion, bf16[1,2048,1024]{2,1,0:T(8,128)(2,1)S(1)} %copy-done.8), kind=kOutput, calls=%fused_computation.14 | convolution fusion | flops 3222798336 | bytes 8912896 | tf_op jit(solution)/shard_map/dot_general | solution.py:134
  95.4 26.8 %all-gather = bf16[32,1,128]{2,1,0:T(2,128)(2,1)S(1)} all-gather(bf16[4,1,128]{2,1,0:T(2,128)(2,1)S(1)} %copy.104), channel_id=2, replica_groups=mesh['ep'=8,'tp'=4] {'ep'}, dimensions={0}, use_global_device_ids=true | all-gather | bytes 9216 | tf_op jit(solution)/shard_map/all_gather | solution.py:13
  122.2 1.8 copy.108
  124.0 2.0 convolution_select_fusion
  126.1 0.6 fusion.28
  126.7 2.0 multiply_reduce_fusion.2
  128.8 0.2 fusion.27
  129.0 1.7 convolution_convert_fusion
  130.7 31.4 %reduce-scatter.5.cloned.1.call-done = bf16[512,768]{0,1:T(8,128)(2,1)} async-done(((bf16[2048,768]{0,1:T(8,128)(2,1)}), bf16[512,768]{0,1:T(8,128)(2,1)}) %reduce-scatter.5.cloned.1.call-update) | async-done | bytes 786448 | tf_op jit(solution)/shard_map/reduce_scatter | solution.py:133
  162.1 5.5 %all-to-all-start.1 = ((bf16[512,8,96]{0,2,1:T(8,128)(2,1)}), bf16[512,8,96]{0,2,1:T(8,128)(2,1)S(1)}, u32[]{:S(2)}, u32[]{:S(2)}) async-start(bf16[512,8,96]{0,2,1:T(8,128)(2,1)} %bitcast.117), calls=%async_computation.3 | async-start | bytes 1572864 | tf_op jit(solution)/shard_map/all_to_all | solution.py:141
  167.8 19.9 %all-to-all-done.1 = bf16[512,8,96]{0,2,1:T(8,128)(2,1)S(1)} async-done(((bf16[512,8,96]{0,2,1:T(8,128)(2,1)}), bf16[512,8,96]{0,2,1:T(8,128)(2,1)S(1)}, u32[]{:S(2)}, u32[]{:S(2)}) %all-to-all-start.1) | async-done | bytes 786464 | tf_op jit(solution)/shard_map/all_to_all | solution.py:141
  187.7 2.6 %gather_fusion.1 = bf16[512,512]{1,0:T(8,128)(2,1)} fusion(bf16[768,512]{1,0:T(8,128)(2,1)S(1)} %bitcast.108, s32[1024]{0:T(1024)S(1)} %pad_clamp_fusion), kind=kCustom, calls=%fused_computation.1 | custom fusion | bytes 1050624 | tf_op jit(solution)/shard_map/gather | solution.py:142
  190.3 1.7 reshape.160
  192.0 2.1 %multiply_reduce_fusion.1 = bf16[256,512]{1,0:T(8,128)(2,1)} fusion(f32[256,2,512]{2,1,0:T(2,128)S(1)} %reshape.160, f32[256,2]{1,0:T(8,128)S(1)} %copy.112), kind=kLoop, calls=%fused_computation.22 | loop fusion | flops 393216 | bytes 1312768 | tf_op jit(solution)/shard_map/reduce_sum | solution.py:143
  (57 shorter events, 1.0 us)
Async XLA Ops:
  7.2 121.8 %copy-start = (bf16[512,2048]{1,0:T(8,128)(2,1)S(1)}, bf16[512,2048]{1,0:T(8,128)(2,1)}, u32[]{:S(2)}) copy-start(bf16[512,2048]{1,0:T(8,128)(2,1)} %param.24) | copy-start | bytes 6291460
  7.2 73.0 %all-gather.5.cloned.1.call-start = ((), (), s32[]{:S(2)}) async-start(), calls=%async_computation.5 | async-start | bytes 3932160 | tf_op jit(solution)/shard_map/all_gather | solution.py:129
  25.0 29.9 %copy-start.6 = (f32[512]{0:T(512)S(1)}, f32[512]{0:T(512)}, u32[]{:S(2)}) copy-start(f32[512]{0:T(512)} %param.21) | copy-start | bytes 6148
  52.5 73.5 %all-gather.7.cloned.1.call-start = ((), (), s32[]{:S(2)}) async-start(), calls=%async_computation.7 | async-start | bytes 1179648 | tf_op jit(solution)/shard_map/all_gather | solution.py:13
  58.1 9.5 %copy-start.2 = (bf16[256,512]{1,0:T(8,128)(2,1)S(1)}, bf16[256,512]{1,0:T(8,128)(2,1)}, u32[]{:S(2)}) copy-start(bf16[256,512]{1,0:T(8,128)(2,1)} %param.19) | copy-start | bytes 786436
  68.9 93.2 %reduce-scatter.5.cloned.1.call-start = ((), (), s32[]{:S(2)}) async-start(), calls=%async_computation.6 | async-start | bytes 3932160 | tf_op jit(solution)/shard_map/reduce_scatter | solution.py:133
  80.2 6.3 %copy-start.7 = (bf16[1,2048,1024]{2,1,0:T(8,128)(2,1)S(1)}, bf16[1,2048,1024]{2,1,0:T(8,128)(2,1)}, u32[]{:S(2)}) copy-start(bf16[1,2048,1024]{2,1,0:T(8,128)(2,1)} %param.29) | copy-start | bytes 12582916
  80.2 6.3 %copy-start.9 = (bf16[768,2048]{1,0:T(8,128)(2,1)S(1)}, bf16[768,2048]{1,0:T(8,128)(2,1)}, u32[]{:S(2)}) copy-start(bf16[768,2048]{1,0:T(8,128)(2,1)} %all-gather.5.cloned.1.call-done) | copy-start | bytes 9437188
  86.5 3.8 %copy-start.8 = (bf16[1,2048,1024]{2,1,0:T(8,128)(2,1)S(1)}, bf16[1,2048,1024]{2,1,0:T(8,128)(2,1)}, u32[]{:S(2)}) copy-start(bf16[1,2048,1024]{2,1,0:T(8,128)(2,1)} %param.31) | copy-start | bytes 12582916
  95.3 28.7 %copy-start.1 = (f32[4,256,128]{2,0,1:T(4,128)S(1)}, f32[4,256,128]{2,0,1:T(4,128)}, u32[]{:S(2)}) copy-start(f32[4,256,128]{2,0,1:T(4,128)} %get-tuple-element.61) | copy-start | bytes 1572868
  95.3 98.8 %reduce-scatter.3.cloned.1.call-start = ((), (), s32[]{:S(2)}) async-start(), calls=%async_computation.4 | async-start | bytes 1310720 | tf_op jit(solution)/shard_map/reduce_scatter | solution.py:82
  126.1 2.7 %copy-start.3 = (bf16[256,512]{0,1:T(8,128)(2,1)S(1)}, bf16[256,512]{0,1:T(8,128)(2,1)}, u32[]{:S(2)}) copy-start(bf16[256,512]{0,1:T(8,128)(2,1)} %copy.108) | copy-start | bytes 786436
  126.1 2.7 %copy-start.4 = (f32[512]{0:T(512)S(1)}, f32[512]{0:T(512)}, u32[]{:S(2)}) copy-start(f32[512]{0:T(512)} %param.23) | copy-start | bytes 6148
  129.0 38.7 %copy-start.5 = (f32[256,2]{0,1:T(2,128)S(1)}, f32[256,2]{0,1:T(2,128)}, u32[]{:S(2)}) copy-start(f32[256,2]{0,1:T(2,128)} %param.28) | copy-start | bytes 6148
  162.1 25.6 %all-to-all-start.1 = ((bf16[512,8,96]{0,2,1:T(8,128)(2,1)}), bf16[512,8,96]{0,2,1:T(8,128)(2,1)S(1)}, u32[]{:S(2)}, u32[]{:S(2)}) async-start(bf16[512,8,96]{0,2,1:T(8,128)(2,1)} %bitcast.117), calls=%async_computation.3 | async-start | bytes 1572864 | tf_op jit(solution)/shard_map/all_to_all | solution.py:141
Sparse Core Ops, SparseCore 0:
  52.6 27.5 all-gather.4
  82.9 40.3 all-gather.6
  125.8 36.2 reduce-scatter.4
  165.1 24.7 reduce-scatter.2
where the time goes:
time: 201 us
  waiting for transfers between devices  62.5 us (31%)
  blocking collectives  54.2 us (27%)
  local copies, waits for them, and re-layouts  25.1 us (12%)
  matrix products  22.6 us (11%)
  other arithmetic  16.3 us (8%)
  between operations  14.1 us (7%)
  starting transfers between devices  5.85 us (3%)
    reduce_scatter x1, waiting for transfers between devices, expert_half(): lax.psum_scatter(lax.dot_general(local_down, hidden, (((1,), (1,)), ((),...  31.4 us
    all_to_all x1, blocking collectives, expert_half(): lax.all_to_all(outgoing, 'ep', split_axis=0, concat_axis=0, tiled=True)  27.3 us
    all_gather x1, blocking collectives, entering(): lax.all_gather(a.astype(kind), axis)  26.8 us
    all_to_all x1, waiting for transfers between devices, expert_half(): lax.all_to_all(summed, 'ep', split_axis=1, concat_axis=1, tiled=True)  19.9 us
    all_gather x1, waiting for transfers between devices, expert_half(): features = lax.all_gather(arrived, 'tp', axis=1, tiled=True)  11.1 us
    unnamed x26, local copies, waits for them, and re-layouts  6.94 us
    dot_general x1, matrix products, expert_half(): up_act = jnp.dot(features, local_up, preferred_element_type=jnp.float32)  6.28 us
    all_to_all x1, starting transfers between devices, expert_half(): lax.all_to_all(summed, 'ep', split_axis=1, concat_axis=1, tiled=True)  5.51 us
  transfers between devices with their start and end apart: 5, of which 3 were waited for; matrix products, arithmetic and copies ran while one was open for 23% of the time, Pallas kernels for 0%

commit v1 on v0

--- a/solution.py
+++ b/solution.py
@@ -126,7 +126,12 @@
     )
     outgoing = jnp.where(filled[:, None], own_columns[owner], jnp.zeros((), jnp.bfloat16))
     arrived = lax.all_to_all(outgoing, "ep", split_axis=0, concat_axis=0, tiled=True)
-    features = lax.all_gather(arrived, "tp", axis=1, tiled=True)
+    ring = [arrived]
+    for hop_ in range(3):
+        ring.append(lax.ppermute(ring[-1], "tp", [(dev, (dev + 1) % 4) for dev in range(4)]))
+    features = jnp.roll(
+        jnp.concatenate(ring[::-1], axis=1), (lax.axis_index("tp") + 1) * ring[0].shape[1], axis=1
+    )
     gate_act = jnp.dot(features, local_gate, preferred_element_type=jnp.float32)
     up_act = jnp.dot(features, local_up, preferred_element_type=jnp.float32)
     hidden = (jax.nn.silu(gate_act) * up_act).astype(jnp.bfloat16)

time: 201 us -> 188 us (0.935)
  waiting for transfers between devices: 62.5 us -> 33 us
  local copies, waits for them, and re-layouts: 25.1 us -> 36.4 us
  other arithmetic: 16.3 us -> 19.4 us
  starting transfers between devices: 5.85 us -> 8.17 us
    reduce_scatter x1, waiting for transfers between devices: 31.4 us -> 2.17 us  [expert_half(): lax.psum_scatter(lax.dot_general(local_down, hidden, (((1,), (1,)), ((),...]
    ppermute x0 -> x3, waiting for transfers between devices: none -> 12.4 us  [expert_half(): lax.ppermute(ring[-1], 'tp', [(dev, (dev + 1) % 4) for dev in range(4)])]
    all_gather x1 -> x0, waiting for transfers between devices: 11.1 us -> none  [expert_half(): features = lax.all_gather(arrived, 'tp', axis=1, tiled=True)]
    unnamed x26 -> x35, local copies, waits for them, and re-layouts: 6.94 us -> 15.2 us
    dot_general x1, matrix products: 6.28 us -> 3.76 us  [expert_half(): up_act = jnp.dot(features, local_up, preferred_element_type=jnp.float32)]
    all_to_all x1, starting transfers between devices: 5.51 us -> 7.86 us  [expert_half(): lax.all_to_all(summed, 'ep', split_axis=1, concat_axis=1, tiled=True)]
  transfers between devices with their start and end apart: 5 -> 7, of which waited for: 3 -> 4; matrix products, arithmetic and copies ran while one was open for 23% -> 31% of each run, Pallas kernels for 0% -> 0%
where the time goes in v1:
time: 188 us; the launch traced here: 187 us
  blocking collectives  53.4 us (28%)
  local copies, waits for them, and re-layouts  36.4 us (19%)
  waiting for transfers between devices  33 us (18%)
  matrix products  20.6 us (11%)
  other arithmetic  19.4 us (10%)
  between operations  15.9 us (8%)
  starting transfers between devices  8.17 us (4%)
    all_to_all x1, blocking collectives, expert_half(): lax.all_to_all(outgoing, 'ep', split_axis=0, concat_axis=0, tiled=True)  27.2 us
    all_gather x1, blocking collectives, entering(): lax.all_gather(a.astype(kind), axis)  26.2 us
    all_to_all x1, waiting for transfers between devices, expert_half(): lax.all_to_all(summed, 'ep', split_axis=1, concat_axis=1, tiled=True)  18.3 us
    unnamed x35, local copies, waits for them, and re-layouts  15.2 us
    ppermute x3, waiting for transfers between devices, expert_half(): lax.ppermute(ring[-1], 'tp', [(dev, (dev + 1) % 4) for dev in range(4)])  12.4 us
    all_to_all x1, starting transfers between devices, expert_half(): lax.all_to_all(summed, 'ep', split_axis=1, concat_axis=1, tiled=True)  7.86 us
    dot_general x1, matrix products, expert_half(): lax.dot_general(local_down, hidden, (((1,), (1,)), ((), ())), preferred_e...  4.88 us
    reshape x2, local copies, waits for them, and re-layouts, by_head(): return array.reshape(tokens, local_heads, HEAD_DIM).transpose(1, 0, 2)  4.09 us
  transfers between devices with their start and end apart: 7, of which 4 were waited for; matrix products, arithmetic and copies ran while one was open for 31% of the time, Pallas kernels for 0%

profile of v1, /device:TPU:0, one launch (start us, length us, event | category | flops | bytes accessed | tf_op | source)
XLA Modules:
  0.0 186.8 jit_solution(7010375598057859188)
XLA Ops:
  8.1 0.9 copy.110
  9.3 0.7 broadcast_multiply_fusion
  10.0 1.4 convert_reduce_fusion
  11.4 2.9 %multiply_reduce_fusion = (f32[256]{0:T(256)S(1)}, f32[256,2048]{1,0:T(8,128)}) fusion(f32[256]{0:T(256)S(1)} %broadcast_multiply_fusion.1, bf16[256,2048]{1,0:T(8,128)(2,1)} %param.25), kind=kLoop, calls=%fused_computation.20 | loop fusion | flops 2096896 | bytes 3147776 | tf_op jit(solution)/shard_map/reduce_sum | solution.py:106
  14.4 1.1 reduce-window.16
  16.2 2.4 %scatter_custom_fusion.1 = s32[768]{0:T(1024)S(1)} fusion(s32[512]{0:T(512)S(1)} %bitcast.121, s32[512]{0:T(512)S(1)} %add_select_fusion, s32[]{:T(128)} %constant.90.clone.1), kind=kCustom, calls=%fused_computation.90 | custom fusion | bytes 3076 | tf_op jit(solution)/shard_map/scatter | solution.py:118
  18.7 2.4 %scatter_custom_fusion = pred[768]{0:T(1024)(128)(4,1)S(1)} fusion(s32[512]{0:T(512)S(1)} %bitcast.122, pred[512]{0:T(512)(128)(4,1)S(1)} %broadcast.136, pred[]{:T(512)} %constant.95.clone.1), kind=kCustom, calls=%fused_computation.94 | custom fusion | bytes 769 | tf_op jit(solution)/shard_map/scatter | solution.py:119
  21.2 0.8 dynamic-slice
  22.0 1.1 fusion.26
  23.1 2.7 %gather_fusion = bf16[768,512]{1,0:T(8,128)(2,1)S(1)} fusion(bf16[256,512]{1,0:T(8,128)(2,1)S(1)} %fusion.26, s32[1024]{0:T(1024)S(1)} %pad_clamp_fusion.1), kind=kCustom, calls=%fused_computation | custom fusion | bytes 1575936 | tf_op jit(solution)/shard_map/gather | solution.py:127
  26.0 27.2 %all_to_all.21 = bf16[8,96,512]{2,1,0:T(8,128)(2,1)S(1)} all-to-all(bf16[8,96,512]{2,1,0:T(8,128)(2,1)S(1)} %broadcast_select_fusion), channel_id=1, replica_groups=mesh['ep'=8,'tp'=4] {'ep'}, dimensions={0} | all-to-all | bytes 1572864 | tf_op jit(solution)/shard_map/all_to_all | solution.py:128
  53.2 1.2 copy.94
  54.5 1.8 copy.93
  56.3 8.5 %collective-permute-done = bf16[768,512]{1,0:T(8,128)(2,1)} collective-permute-done((bf16[768,512]{1,0:T(8,128)(2,1)S(1)}, bf16[768,512]{1,0:T(8,128)(2,1)}, u32[]{:S(2)}, u32[]{:S(2)}) %collective-permute-start) | collective-permute-done | bytes 786464 | tf_op jit(solution)/shard_map/ppermute | solution.py:131
  64.8 2.3 %divide_multiply_fusion = (f32[256,512]{0,1:T(8,128)}, f32[256,512]{0,1:T(8,128)}) fusion(bf16[256,512]{0,1:T(8,128)(2,1)} %copy.93, f32[512]{0:T(512)S(1)} %copy-done.7, f32[256,512]{0,1:T(8,128)S(1)} %copy.94), kind=kLoop, calls=%fused_computation.52 | loop fusion | flops 786432 | bytes 1837056 | tf_op jit(solution)/shard_map/mul | solution.py:48
  67.0 2.1 %copy.95 = f32[4,128,256]{1,2,0:T(8,128)} copy(f32[4,128,256]{2,1,0:T(8,128)} %bitcast.116) | data formatting | bytes 1048576 | tf_op jit(solution)/shard_map/transpose
  69.1 1.5 fusion.29
  70.6 1.8 copy.91
  72.6 3.9 %collective-permute-done.1 = bf16[768,512]{1,0:T(8,128)(2,1)} collective-permute-done((bf16[768,512]{1,0:T(8,128)(2,1)}, bf16[768,512]{1,0:T(8,128)(2,1)}, u32[]{:S(2)}, u32[]{:S(2)}) %collective-permute-start.1) | collective-permute-done | bytes 786464 | tf_op jit(solution)/shard_map/ppermute | solution.py:131
  76.5 1.9 %convert_multiply_fusion.1 = f32[256,512]{0,1:T(8,128)} fusion(bf16[256,512]{0,1:T(8,128)(2,1)} %copy.91), kind=kLoop, calls=%fused_computation.28 | loop fusion | flops 655360 | bytes 786432 | tf_op jit(solution)/shard_map/jit(silu)/mul | solution.py:50
  78.4 1.2 copy.146
  79.6 2.0 %copy.99 = f32[256,4,128]{2,1,0:T(4,128)} copy(f32[256,4,128]{0,2,1:T(8,128)} %bitcast.115) | data formatting | bytes 1048576 | tf_op jit(solution)/shard_map/reshape | solution.py:54
  81.6 2.1 %copy.92 = f32[256,4,128]{2,1,0:T(4,128)} copy(f32[256,4,128]{0,2,1:T(8,128)} %bitcast.113) | data formatting | bytes 1048576 | tf_op jit(solution)/shard_map/reshape | solution.py:54
  83.7 0.6 slice_bitcast_fusion.1
  84.3 2.9 %bitcast_multiply_fusion.3 = (f32[4,256,128]{2,0,1:T(4,128)}, f32[4,256,128]{2,0,1:T(4,128)S(1)}, f32[4,256,128]{2,0,1:T(4,128)}) fusion(f32[256,4,128]{2,1,0:T(4,128)} %copy.99, f32[4,128,256]{1,2,0:T(8,128)S(1)} %bitcast.111, f32[4,128]{1,0:T(4,128)S(1)} %get-tuple-element.64, f32[256,4,128]{2,1,0:T(4,128)} %copy.92), kind=kLoop, calls=%fused_computation.43 | loop fusion | flops 655360 | bytes 3147776 | tf_op jit(solution)/shard_map/mul | solution.py:64
  87.2 2.3 %convolution_convert_fusion.1 = bf16[4,128,128]{2,1,0:T(8,128)(2,1)} fusion(f32[4,256,128]{2,0,1:T(4,128)S(1)} %get-tuple-element.62, bf16[256,512]{1,0:T(8,128)(2,1)} %param.19), kind=kOutput, calls=%fused_computation.23 | convolution fusion | flops 201392128 | bytes 917504 | tf_op jit(solution)/shard_map/htd,htv->hdv/dot_general | solution.py:71
  89.5 0.2 reduce-scatter.5.cloned.1.call-start
  89.7 1.2 constant_dynamic-update-slice_fusion.7
  91.0 1.2 constant_dynamic-update-slice_fusion.6
  92.2 1.2 constant_dynamic-update-slice_fusion.5
  93.5 1.4 constant_dynamic-update-slice_fusion.3
  94.9 1.2 constant_dynamic-update-slice_fusion.2
  96.2 1.2 constant_dynamic-update-slice_fusion.1
  97.5 3.4 %fusion.4 = f32[768,1024]{1,0:T(8,128)S(1)} fusion(bf16[1,2048,1024]{2,1,0:T(8,128)(2,1)S(1)} %copy-done.8, bf16[768,4096]{1,0:T(8,128)(2,1)S(1)} %constant_dynamic-update-slice_fusion, s32[]{:T(128)S(6)} %select_n.59), kind=kOutput, calls=%fused_computation.10 | convolution fusion | flops 3221225472 | bytes 10485764 | tf_op jit(solution)/shard_map/dot_general | solution.py:135
  101.0 3.8 %multiply_convert_fusion = bf16[768,1024]{1,0:T(8,128)(2,1)S(1)} fusion(f32[768,1024]{1,0:T(8,128)S(1)} %fusion.4, bf16[1,2048,1024]{2,1,0:T(8,128)(2,1)S(1)} %copy-done.9, bf16[768,4096]{1,0:T(8,128)(2,1)S(1)} %constant_dynamic-update-slice_fusion, s32[]{:T(128)S(6)} %select_n.59), kind=kOutput, calls=%fused_computation.13 | convolution fusion | flops 3225944064 | bytes 12058628 | tf_op jit(solution)/shard_map/dot_general | solution.py:136
  104.8 4.9 %fusion.9 = bf16[2048,768]{0,1:T(8,128)(2,1)} fusion(bf16[768,1024]{1,0:T(8,128)(2,1)S(1)} %multiply_convert_fusion, bf16[1,2048,1024]{2,1,0:T(8,128)(2,1)S(1)} %copy-done.10), kind=kOutput, calls=%fused_computation.14 | convolution fusion | flops 3222798336 | bytes 8912896 | tf_op jit(solution)/shard_map/dot_general | solution.py:139
  109.8 26.2 %all-gather = bf16[32,1,128]{2,1,0:T(2,128)(2,1)S(1)} all-gather(bf16[4,1,128]{2,1,0:T(2,128)(2,1)S(1)} %copy.104), channel_id=2, replica_groups=mesh['ep'=8,'tp'=4] {'ep'}, dimensions={0}, use_global_device_ids=true | all-gather | bytes 9216 | tf_op jit(solution)/shard_map/all_gather | solution.py:13
  135.9 1.8 copy.108
  137.8 2.0 %convolution_select_fusion = f32[4,256,256]{2,1,0:T(8,128)} fusion(f32[4,256,128]{2,0,1:T(4,128)S(1)} %copy-done.2, pred[256,256]{1,0:T(8,128)(4,1)S(1)} %iota_compare_fusion, f32[4,256,128]{2,0,1:T(4,128)S(1)} %copy-done.1), kind=kOutput, calls=%fused_computation.21 | convolution fusion | flops 402915328 | bytes 2162688 | tf_op jit(solution)/shard_map/htd,hsd->hts/dot_general | solution.py:65
  139.8 0.6 fusion.32
  140.5 2.0 %multiply_reduce_fusion.2 = (f32[4,256]{1,0:T(4,128)S(1)}, f32[4,256,128]{1,2,0:T(8,128)S(1)}) fusion(f32[4,256,128]{1,2,0:T(8,128)S(1)} %fusion.32, f32[4,256,256]{2,1,0:T(8,128)} %convolution_select_fusion, bf16[256,512]{1,0:T(8,128)(2,1)S(1)} %copy-done.3), kind=kOutput, calls=%fused_computation.50 | convolution fusion | flops 403045376 | bytes 2363392 | tf_op jit(solution)/shard_map/hts,hsv->htv/dot_general | solution.py:68
  142.7 1.7 convolution_convert_fusion
  144.5 2.2 %reduce-scatter.5.cloned.1.call-done = bf16[512,768]{0,1:T(8,128)(2,1)} async-done(((bf16[2048,768]{0,1:T(8,128)(2,1)}), bf16[512,768]{0,1:T(8,128)(2,1)}) %reduce-scatter.5.cloned.1.call-update) | async-done | bytes 786448 | tf_op jit(solution)/shard_map/reduce_scatter | solution.py:138
  146.6 7.9 %all-to-all-start.1 = ((bf16[512,8,96]{0,2,1:T(8,128)(2,1)}), bf16[512,8,96]{0,2,1:T(8,128)(2,1)S(1)}, u32[]{:S(2)}, u32[]{:S(2)}) async-start(bf16[512,8,96]{0,2,1:T(8,128)(2,1)} %bitcast.117), calls=%async_computation.3 | async-start | bytes 1572864 | tf_op jit(solution)/shard_map/all_to_all | solution.py:146
  154.7 18.3 %all-to-all-done.1 = bf16[512,8,96]{0,2,1:T(8,128)(2,1)S(1)} async-done(((bf16[512,8,96]{0,2,1:T(8,128)(2,1)}), bf16[512,8,96]{0,2,1:T(8,128)(2,1)S(1)}, u32[]{:S(2)}, u32[]{:S(2)}) %all-to-all-start.1) | async-done | bytes 786464 | tf_op jit(solution)/shard_map/all_to_all | solution.py:146
  173.0 2.6 %gather_fusion.1 = bf16[512,512]{1,0:T(8,128)(2,1)} fusion(bf16[768,512]{1,0:T(8,128)(2,1)S(1)} %bitcast.106, s32[1024]{0:T(1024)S(1)} %pad_clamp_fusion), kind=kCustom, calls=%fused_computation.1 | custom fusion | bytes 1050624 | tf_op jit(solution)/shard_map/gather | solution.py:147
  175.7 1.7 reshape.160
  177.4 2.1 %multiply_reduce_fusion.1 = bf16[256,512]{1,0:T(8,128)(2,1)} fusion(f32[256,2,512]{2,1,0:T(2,128)S(1)} %reshape.160, f32[256,2]{1,0:T(8,128)S(1)} %copy.112), kind=kLoop, calls=%fused_computation.24 | loop fusion | flops 393216 | bytes 1312768 | tf_op jit(solution)/shard_map/reduce_sum | solution.py:148
  (70 shorter events, 2.3 us)
Async XLA Ops:
  8.0 134.7 %copy-start = (bf16[512,2048]{1,0:T(8,128)(2,1)S(1)}, bf16[512,2048]{1,0:T(8,128)(2,1)}, u32[]{:S(2)}) copy-start(bf16[512,2048]{1,0:T(8,128)(2,1)} %param.24) | copy-start | bytes 6291460
  8.0 131.8 %all-gather.4.cloned.1.call-start = ((), (), s32[]{:S(2)}) async-start(), calls=%async_computation.6 | async-start | bytes 1179648 | tf_op jit(solution)/shard_map/all_gather | solution.py:13
  23.1 41.6 %copy-start.7 = (f32[512]{0:T(512)S(1)}, f32[512]{0:T(512)}, u32[]{:S(2)}) copy-start(f32[512]{0:T(512)} %param.21) | copy-start | bytes 6148
  53.2 11.5 %collective-permute-start = (bf16[768,512]{1,0:T(8,128)(2,1)S(1)}, bf16[768,512]{1,0:T(8,128)(2,1)}, u32[]{:S(2)}, u32[]{:S(2)}) collective-permute-start(bf16[768,512]{1,0:T(8,128)(2,1)S(1)} %bitcast.107), channel_id=1, source_target_pairs={{0,1},{1,2},{2,3},{3,0},{4,5},{5,6},{6,7},{7,4},{8,9},{9,10},{10,1... | collective-permute-start | bytes 2359304 | tf_op jit(solution)/shard_map/ppermute | solution.py:131
  64.8 11.7 %collective-permute-start.1 = (bf16[768,512]{1,0:T(8,128)(2,1)}, bf16[768,512]{1,0:T(8,128)(2,1)}, u32[]{:S(2)}, u32[]{:S(2)}) collective-permute-start(bf16[768,512]{1,0:T(8,128)(2,1)} %collective-permute-done), channel_id=1, source_target_pairs={{0,1},{1,2},{2,3},{3,0},{4,5},{5,6},{6,7},{7,4},{8,9},{9,10},{10,1... | collective-permute-start | bytes 2359304 | tf_op jit(solution)/shard_map/ppermute | solution.py:131
  76.5 13.2 %collective-permute-start.2 = (bf16[768,512]{1,0:T(8,128)(2,1)}, bf16[768,512]{1,0:T(8,128)(2,1)}, u32[]{:S(2)}, u32[]{:S(2)}) collective-permute-start(bf16[768,512]{1,0:T(8,128)(2,1)} %collective-permute-done.1), channel_id=1, source_target_pairs={{0,1},{1,2},{2,3},{3,0},{4,5},{5,6},{6,7},{7,4},{8,9},{9,10},{10,1... | collective-permute-start | bytes 2359304 | tf_op jit(solution)/shard_map/ppermute | solution.py:131
  89.5 57.2 %reduce-scatter.5.cloned.1.call-start = ((), (), s32[]{:S(2)}) async-start(), calls=%async_computation.5 | async-start | bytes 3932160 | tf_op jit(solution)/shard_map/reduce_scatter | solution.py:138
  93.4 4.1 %copy-start.8 = (bf16[1,2048,1024]{2,1,0:T(8,128)(2,1)S(1)}, bf16[1,2048,1024]{2,1,0:T(8,128)(2,1)}, u32[]{:S(2)}) copy-start(bf16[1,2048,1024]{2,1,0:T(8,128)(2,1)} %param.29) | copy-start | bytes 12582916
  97.5 3.4 %copy-start.9 = (bf16[1,2048,1024]{2,1,0:T(8,128)(2,1)S(1)}, bf16[1,2048,1024]{2,1,0:T(8,128)(2,1)}, u32[]{:S(2)}) copy-start(bf16[1,2048,1024]{2,1,0:T(8,128)(2,1)} %param.30) | copy-start | bytes 12582916
  101.0 3.8 %copy-start.10 = (bf16[1,2048,1024]{2,1,0:T(8,128)(2,1)S(1)}, bf16[1,2048,1024]{2,1,0:T(8,128)(2,1)}, u32[]{:S(2)}) copy-start(bf16[1,2048,1024]{2,1,0:T(8,128)(2,1)} %param.31) | copy-start | bytes 12582916
  104.8 33.0 %copy-start.1 = (f32[4,256,128]{2,0,1:T(4,128)S(1)}, f32[4,256,128]{2,0,1:T(4,128)}, u32[]{:S(2)}) copy-start(f32[4,256,128]{2,0,1:T(4,128)} %get-tuple-element.63) | copy-start | bytes 1572868
  104.8 33.0 %copy-start.2 = (f32[4,256,128]{2,0,1:T(4,128)S(1)}, f32[4,256,128]{2,0,1:T(4,128)}, u32[]{:S(2)}) copy-start(f32[4,256,128]{2,0,1:T(4,128)} %get-tuple-element.61) | copy-start | bytes 1572868
  109.7 30.8 %copy-start.3 = (bf16[256,512]{1,0:T(8,128)(2,1)S(1)}, bf16[256,512]{1,0:T(8,128)(2,1)}, u32[]{:S(2)}) copy-start(bf16[256,512]{1,0:T(8,128)(2,1)} %param.19) | copy-start | bytes 786436
  109.7 69.7 %reduce-scatter.3.cloned.1.call-start = ((), (), s32[]{:S(2)}) async-start(), calls=%async_computation.4 | async-start | bytes 1310720 | tf_op jit(solution)/shard_map/reduce_scatter | solution.py:82
  139.8 2.7 %copy-start.4 = (bf16[256,512]{0,1:T(8,128)(2,1)S(1)}, bf16[256,512]{0,1:T(8,128)(2,1)}, u32[]{:S(2)}) copy-start(bf16[256,512]{0,1:T(8,128)(2,1)} %copy.108) | copy-start | bytes 786436
  139.8 2.7 %copy-start.5 = (f32[512]{0:T(512)S(1)}, f32[512]{0:T(512)}, u32[]{:S(2)}) copy-start(f32[512]{0:T(512)} %param.23) | copy-start | bytes 6148
  142.4 12.1 %copy-start.6 = (f32[256,2]{0,1:T(2,128)S(1)}, f32[256,2]{0,1:T(2,128)}, u32[]{:S(2)}) copy-start(f32[256,2]{0,1:T(2,128)} %param.28) | copy-start | bytes 6148
  146.6 26.4 %all-to-all-start.1 = ((bf16[512,8,96]{0,2,1:T(8,128)(2,1)}), bf16[512,8,96]{0,2,1:T(8,128)(2,1)S(1)}, u32[]{:S(2)}, u32[]{:S(2)}) async-start(bf16[512,8,96]{0,2,1:T(8,128)(2,1)} %bitcast.117), calls=%async_computation.3 | async-start | bytes 1572864 | tf_op jit(solution)/shard_map/all_to_all | solution.py:146
Sparse Core Ops, SparseCore 0:
  89.6 39.6 all-gather.3
Sparse Core Ops, SparseCore 1:
  109.8 36.8 reduce-scatter.4
  149.6 25.1 reduce-scatter.2
